TPU v7x, 256 devices: a whole 4x4x8 slice. The times are simulated.
256 devices in a mesh: sp: 64 (over z, y, core), tp: 4 (over x).
Axes of the slice: x: 4, y: 4, z: 8, core: 2. Of those that a mesh axis runs over, the one named last changes fastest.
Arguments:
- stream: bfloat16 [65536, 4096], P('sp', 'tp'), may hold values from -11 to 11
- norm_gain: bfloat16 [3, 4096], P(None, 'tp'), may hold values from 0.099609375 to 1.8984375
- pool_weight: bfloat16 [3, 4, 1024, 1024], P(None, 'tp', 'sp'), may hold values from -0.1875 to 0.1875
- pool_scale: bfloat16 [3, 4096], P(None, 'tp'), may hold values from 0.099609375 to 1.8984375
Outputs:
- mixed: bfloat16 [65536, 4096], P('sp', 'tp')
All inputs are finite; a program needn't handle non-finite values.
Results may differ from a plain program's by a relative error of at most 0.015.
Values may be sent and summed in bfloat16 or wider, within the bound.
A program may use at most 64 MiB of HBM per device.

v0:
```python
import functools

import jax
import jax.numpy as jnp
from jax import lax
from jax.experimental import pallas as pl
from jax.experimental.pallas import tpu as pltpu
from jax.sharding import PartitionSpec as P

D = 4096
POOL_GROUPS = 4
NORM_EPS = 1e-06
PAD = 64
HALO = 32
TILE = 128
DOWN, UP, ACROSS = 0, 1, 2
MESH = pl.DeviceIdType.MESH


LEAD, SKEW, EARLY = 5, 3, 2
MIX_AT = 6


def unit_list(layers, width):
    eighth = width // 8
    units = []
    for layer in range(layers):
        sizes = [3, 2, 2] if layer == layers - 1 else [2, 2, 3]
        units.append((layer, 7 * eighth, eighth, True))
        first = 0
        for size in sizes:
            units.append((layer, first * eighth, size * eighth, False))
            first += size
    return units


def kernel(cfg, x_hbm, w_hbm, gain_hbm, scale_hbm, out_ref, gain_ref, scale_ref, xs, ns, ps, ws, ss_own, ss_in,
           load_sem, halo_send, halo_recv, ss_send, ss_recv, w_send, w_recv, out_sem):
    layers, rows, width, shard_rows, n_sp, n_tp, in_kernel = cfg
    sp, tp = lax.axis_index("sp"), lax.axis_index("tp")
    line = n_sp // 2
    z, y = sp // 2, sp % 2
    units = unit_list(layers, width)
    total_rows = rows + 2 * PAD
    tiles = total_rows // TILE
    seq_total = rows * n_sp
    base_pos = sp * rows - PAD
    half = jnp.left_shift(jnp.int32(1), tp)

    has_down, has_up = z > 0, z < line - 1
    has_prev, has_next = sp > 0, sp < n_sp - 1
    target = {DOWN: (sp - 2, tp), UP: (sp + 2, tp), ACROSS: (z * 2 + (1 - y), tp)}

    x_load = pltpu.make_async_copy(x_hbm, xs.at[pl.ds(PAD, rows)], load_sem.at[layers])
    own_rows = pl.ds(pl.multiple_of(sp * shard_rows, shard_rows), shard_rows)
    if in_kernel:
        w_loads = [
            pltpu.make_async_copy(w_hbm.at[l, 0], ws.at[l, own_rows], load_sem.at[l])
            for l in range(layers)
        ]
    else:
        w_loads = [
            pltpu.make_async_copy(w_hbm.at[l, 0], ws.at[l], load_sem.at[l])
            for l in range(layers)
        ]
    w_loads[0].start()
    x_load.start()
    gain_load = pltpu.make_async_copy(gain_hbm, gain_ref, load_sem.at[layers + 1])
    scale_load = pltpu.make_async_copy(scale_hbm, scale_ref, load_sem.at[layers + 2])
    gain_load.start()
    scale_load.start()
    for l in range(1, layers):
        w_loads[l].start()

    barrier = pltpu.get_barrier_semaphore()

    def greet(device):
        pl.semaphore_signal(barrier, inc=1, device_id=device, device_id_type=MESH)

    expected = jnp.int32(n_tp - 1)
    for p in range(1, n_tp):
        greet((sp, lax.rem(tp + p, n_tp)))
    pl.when(has_prev)(lambda: greet((sp - 1, tp)))
    pl.when(has_next)(lambda: greet((sp + 1, tp)))
    expected = expected + has_prev.astype(jnp.int32) + has_next.astype(jnp.int32)
    if in_kernel:
        greet(target[ACROSS])
        pl.when(has_down)(lambda: greet(target[DOWN]))
        pl.when(has_up)(lambda: greet(target[UP]))
        expected = expected + 1 + has_down.astype(jnp.int32) + has_up.astype(jnp.int32)

    zero = jnp.zeros((PAD, width), jnp.bfloat16)
    ns[pl.ds(0, PAD)] = zero
    ns[pl.ds(total_rows + PAD, PAD)] = zero
    xs[pl.ds(0, PAD - HALO)] = zero[: PAD - HALO]
    xs[pl.ds(PAD + rows + HALO, PAD - HALO)] = zero[: PAD - HALO]

    @pl.when(jnp.logical_not(has_prev))
    def _():
        xs[pl.ds(PAD - HALO, HALO)] = zero[:HALO]

    @pl.when(jnp.logical_not(has_next))
    def _():
        xs[pl.ds(PAD + rows, HALO)] = zero[:HALO]

    pl.semaphore_wait(barrier, expected)

    to_next = pltpu.make_async_remote_copy(
        x_hbm.at[pl.ds(rows - HALO, HALO)], xs.at[pl.ds(PAD - HALO, HALO)],
        halo_send.at[0], halo_recv.at[0], device_id=(sp + 1, tp), device_id_type=MESH)
    to_prev = pltpu.make_async_remote_copy(
        x_hbm.at[pl.ds(0, HALO)], xs.at[pl.ds(PAD + rows, HALO)],
        halo_send.at[1], halo_recv.at[1], device_id=(sp - 1, tp), device_id_type=MESH)
    pl.when(has_next)(lambda: to_next.start())
    pl.when(has_prev)(lambda: to_prev.start())

    def piece(u, j, col):
        layer, first, columns, _ = units[u]
        start = pl.multiple_of((j * 2 + col) * shard_rows, shard_rows)
        return ws.at[layer, pl.ds(start, shard_rows), pl.ds(first, columns)]

    def copy(way, u, j, col):
        at = j * 2 + col
        return pltpu.make_async_remote_copy(
            piece(u, j, col), piece(u, j, col), w_send.at[way, u, at], w_recv.at[u, at],
            device_id=target[way], device_id_type=MESH)

    def arrive(u, j, col):
        copy(ACROSS, u, j, col).wait_recv()

    def send_own(u):
        pl.when(has_down)(lambda: copy(DOWN, u, z, y).start())
        pl.when(has_up)(lambda: copy(UP, u, z, y).start())
        copy(ACROSS, u, z, y).start()

    def pass_own_row(u):
        arrive(u, z, 1 - y)
        pl.when(has_down)(lambda: copy(DOWN, u, z, 1 - y).start())
        pl.when(has_up)(lambda: copy(UP, u, z, 1 - y).start())

    def forward(u, step):
        along = units[u][3]

        def hop(j, way, more):
            arrive(u, j, y)
            pl.when(more)(lambda: copy(way, u, j, y).start())
            if along:
                arrive(u, j, 1 - y)
                pl.when(more)(lambda: copy(way, u, j, 1 - y).start())
            else:
                copy(ACROSS, u, j, y).start()

        pl.when(z + step < line)(lambda: hop(z + step, DOWN, has_down))
        pl.when(z - step >= 0)(lambda: hop(z - step, UP, has_up))

    def arrive_across(u):
        if not units[u][3]:
            for j in range(line):
                arrive(u, j, 1 - y)

    def tile_rows(i):
        return pl.ds(pl.multiple_of(i * TILE, TILE), TILE)

    def square_sums(layer):
        @pl.loop(0, tiles)
        def _(i):
            part = jnp.zeros((TILE, 128), jnp.float32)
            for c in range(width // 128):
                v = xs[tile_rows(i), pl.ds(c * 128, 128)].astype(jnp.float32)
                part = part + v * v
            ss_own[layer, pl.ds(i, 1)] = jnp.sum(part.T, axis=0, keepdims=True)

    def ss_copy(layer, p):
        return pltpu.make_async_remote_copy(
            ss_own.at[layer], ss_in.at[layer, p - 1], ss_send.at[layer, p - 1], ss_recv.at[layer, p - 1],
            device_id=(sp, lax.rem(tp + p, n_tp)), device_id_type=MESH)

    def send_sums(layer):
        square_sums(layer)
        for p in range(1, n_tp):
            ss_copy(layer, p).start()

    def wait_sums(layer):
        for p in range(1, n_tp):
            ss_copy(layer, p).wait()

    def normalise(layer, lo, hi):
        @pl.loop(lo, hi)
        def _(i):
            total = ss_own[layer, pl.ds(i, 1)]
            for p in range(1, n_tp):
                total = total + ss_in[layer, p - 1, pl.ds(i, 1)]
            factor = lax.rsqrt(total / D + NORM_EPS)
            pos = base_pos + i * TILE + lax.broadcasted_iota(jnp.int32, (1, TILE), 1)
            factor = jnp.where((pos >= 0) & (pos < seq_total), factor, 0.0)
            column = jnp.broadcast_to(factor, (TILE, TILE)).T
            for c in range(width // 128):
                cols = pl.ds(c * 128, 128)
                v = xs[tile_rows(i), cols].astype(jnp.float32)
                g = gain_ref[layer : layer + 1, cols].astype(jnp.float32)
                ns[pl.ds(pl.multiple_of(PAD + i * TILE, 64), TILE), cols] = (v * column * g).astype(jnp.bfloat16)

    window = TILE + 2 * PAD

    def pool(lo, hi):
        @pl.loop(lo, hi)
        def _(i):
            offset = (
                lax.broadcasted_iota(jnp.int32, (TILE, window), 1)
                - lax.broadcasted_iota(jnp.int32, (TILE, window), 0)
                - PAD
            )
            pos = base_pos + i * TILE + lax.broadcasted_iota(jnp.int32, (TILE, window), 0)
            count = jnp.minimum(pos + half, seq_total) - jnp.maximum(pos - half, 0)
            count = jnp.maximum(count, 1).astype(jnp.float32)
            band = jnp.where((offset >= -half) & (offset < half), 1.0, 0.0)
            band = (band - jnp.where(offset == 0, count, 0.0)).astype(jnp.bfloat16)
            inverse = 1.0 / count[:, :1]
            rows_in = pl.ds(pl.multiple_of(i * TILE, TILE), window)
            for c in range(width // 256):
                cols = pl.ds(c * 256, 256)
                sums = jnp.dot(band, ns[rows_in, cols], preferred_element_type=jnp.float32)
                ps[tile_rows(i), cols] = (sums * inverse).astype(jnp.bfloat16)

    def mix(layer, first_row, block, first, columns):
        cols = pl.ds(first, columns)
        at = pl.ds(pl.multiple_of(first_row, 64), block)
        branch = jnp.dot(ps[at], ws[layer, :, cols], preferred_element_type=jnp.float32)
        s = scale_ref[layer : layer + 1, cols].astype(jnp.float32)
        mixed = (xs[at, cols].astype(jnp.float32) + branch * s).astype(jnp.bfloat16)
        xs[at, cols] = mixed

    third = tiles // 3
    thirds = [(0, third), (third, 2 * third), (2 * third, tiles)]

    def mix_block(layer, lo, hi):
        def run():
            for c in range(width // 256):
                mix(layer, lo * TILE, (hi - lo) * TILE, c * 256, 256)
        return run

    def prepare(layer):
        work = [lambda: send_sums(layer), lambda: None]
        first = [True]

        def norm(lo, hi):
            if first[0]:
                wait_sums(layer)
                first[0] = False
            normalise(layer, lo, hi)

        work += [functools.partial(norm, lo, hi) for lo, hi in thirds]
        work += [functools.partial(pool, lo, hi) for lo, hi in thirds]
        return work

    def start_work():
        x_load.wait()
        gain_load.wait()
        scale_load.wait()
        pl.when(has_prev)(lambda: to_next.wait_recv())
        pl.when(has_next)(lambda: to_prev.wait_recv())

    if in_kernel:
        w_loads[0].wait()
        loaded = [0]

        def own(u):
            if units[u][0] > loaded[0]:
                loaded[0] = units[u][0]
                w_loads[loaded[0]].wait()
            send_own(u)

        tasks = [start_work] + prepare(0)

        def next_layer(layer):
            while tasks:
                tasks.pop(0)()
            for v in range(len(units)):
                if units[v][0] == layer - 1:
                    arrive_across(v)
            tasks.extend([mix_block(layer - 1, lo, hi) for lo, hi in thirds] + prepare(layer))

        events = []
        place = 0
        for u in range(len(units)):
            events.append((place - LEAD, 0, u, functools.partial(own, u)))
            if units[u][3]:
                events.append((place - EARLY, 1, u, functools.partial(pass_own_row, u)))
            for step in range(1, line):
                events.append((place + SKEW * (step - 1), 2 + step, u, functools.partial(forward, u, step)))
            place += units[u][2] // (width // 8)
        for layer in range(1, layers):
            events.append((8 * layer + MIX_AT, 2, 0, functools.partial(next_layer, layer)))
        for _, kind, _, event in sorted(events, key=lambda e: e[:3]):
            event()
            if kind > 2 and tasks:
                tasks.pop(0)()
        while tasks:
            tasks.pop(0)()
    else:
        start_work()
        for layer in range(layers):
            for task in prepare(layer):
                task()
            w_loads[layer].wait()
            if layer < layers - 1:
                for lo, hi in thirds:
                    mix_block(layer, lo, hi)()

    outs = []
    for u, (layer, first, columns, _) in enumerate(units):
        if layer < layers - 1:
            continue
        if in_kernel:
            arrive_across(u)

        @pl.loop(0, rows // 256)
        def _(i):
            mix(layer, PAD + i * 256, 256, first, columns)

        outs.append(pltpu.make_async_copy(
            xs.at[pl.ds(PAD, rows), pl.ds(first, columns)], out_ref.at[:, pl.ds(first, columns)], out_sem.at[len(outs)]))
        outs[-1].start()

    pl.when(has_next)(lambda: to_next.wait_send())
    pl.when(has_prev)(lambda: to_prev.wait_send())
    if in_kernel:
        for u in range(len(units)):
            along = units[u][3]
            for j in range(line):
                def done(way, col):
                    copy(way, u, j, col).wait_send()

                @pl.when(has_down & (j >= z))
                def _():
                    done(DOWN, y)
                    if along:
                        done(DOWN, 1 - y)

                @pl.when(has_up & (j <= z))
                def _():
                    done(UP, y)
                    if along:
                        done(UP, 1 - y)

                if along:
                    pl.when(z == j)(lambda: done(ACROSS, y))
                else:
                    done(ACROSS, y)
    for out in outs:
        out.wait()


def solution(mesh):
    n_sp, n_tp = mesh.shape["sp"], mesh.shape["tp"]
    in_kernel = n_sp % 2 == 0 and n_sp <= 16

    def local(stream, norm_gain, pool_weight, pool_scale):
        rows, _ = stream.shape
        layers, per_dev, shard_rows, width = pool_weight.shape
        assert per_dev == 1 and n_tp == POOL_GROUPS
        if not in_kernel:
            pool_weight = lax.all_gather(pool_weight, "sp", axis=2, tiled=True)
        total_rows = rows + 2 * PAD
        units = len(unit_list(layers, width)) if in_kernel else 1
        dma = pltpu.SemaphoreType.DMA
        hbm = pl.BlockSpec(memory_space=pltpu.HBM)
        return pl.pallas_call(
            functools.partial(kernel, (layers, rows, width, shard_rows, n_sp, n_tp, in_kernel)),
            out_shape=jax.ShapeDtypeStruct((rows, width), jnp.bfloat16),
            in_specs=[hbm] * 4,
            out_specs=hbm,
            scratch_shapes=[
                pltpu.VMEM((layers, width), jnp.bfloat16),
                pltpu.VMEM((layers, width), jnp.bfloat16),
                pltpu.VMEM((total_rows, width), jnp.bfloat16),
                pltpu.VMEM((total_rows + 2 * PAD, width), jnp.bfloat16),
                pltpu.VMEM((total_rows, width), jnp.bfloat16),
                pltpu.VMEM((layers, width, width), jnp.bfloat16),
                pltpu.VMEM((layers, 16, TILE), jnp.float32),
                pltpu.VMEM((layers, n_tp - 1, 16, TILE), jnp.float32),
                dma((layers + 3,)),
                dma((2,)),
                dma((2,)),
                dma((layers, n_tp - 1)),
                dma((layers, n_tp - 1)),
                dma((3, units, n_sp)),
                dma((units, n_sp)),
                dma((4,)),
            ],
            compiler_params=pltpu.CompilerParams(
                collective_id=0, has_side_effects=True, vmem_limit_bytes=60 * 2**20
            ),
        )(stream, pool_weight, norm_gain, pool_scale)

    placed = (P("sp", "tp"), P(None, "tp"), P(None, "tp", "sp", None), P(None, "tp"))
    return jax.shard_map(
        local, mesh=mesh, in_specs=placed, out_specs=P("sp", "tp"), check_vma=False
    )
```

profile of v0, /device:TPU:1, one launch (start us, length us, event | category | flops | bytes accessed | tf_op | source)
XLA Modules:
  0.0 145.9 jit_solution(6341895537867099498)
XLA Ops:
  6.5 0.0 all-gather.2.cloned.1.call-start
  6.5 0.7 all-gather.2.cloned.1.call-update
  7.3 87.7 %all-gather.2.cloned.1.call-done.w_hbm = bf16[3,1,1024,1024]{3,2,1,0:T(8,128)(2,1)} async-done(((bf16[3,1,16,1024]{3,2,1,0:T(8,128)(2,1)}), bf16[3,1,1024,1024]{3,2,1,0:T(8,128)(2,1)}) %all-gather.2.cloned.1.call-update) | async-done | bytes 6291472 | tf_op jit(solution)/shard_map/all_gather | solution.py:363
  94.9 41.0 %shard_map.46 = bf16[1024,1024]{1,0:T(8,128)(2,1)} custom-call(bf16[1024,1024]{1,0:T(8,128)(2,1)} %x_hbm.1, bf16[3,1,1024,1024]{3,2,1,0:T(8,128)(2,1)} %all-gather.2.cloned.1.call-done.w_hbm, bf16[3,1024]{1,0:T(4,128)(2,1)} %gain_hbm.1, bf16[3,1024]{1,0:T(4,128)(2,1)} %scale_hbm.1), custom_call_target="tpu_custom_call" | custom-call | tf_op jit(solution)/shard_map/pallas_call | solution.py:368
  136.0 3.1 %copy.6 = bf16[1024,1024]{1,0:T(8,128)(2,1)} copy(bf16[1024,1024]{1,0:T(8,128)(2,1)} %shard_map.46) | data formatting | bytes 4194304
Async XLA Ops:
  6.5 88.4 %all-gather.2.cloned.1.call-start = ((), (), s32[]{:S(2)}) async-start(), calls=%async_computation | async-start | bytes 6389760 | tf_op jit(solution)/shard_map/all_gather | solution.py:363
Sparse Core Ops, SparseCore 0:
  10.1 84.7 all-gather.1
where the time goes:
time: 149 us; the launch traced here: 146 us
  waiting for transfers between devices  88.4 us (59%)
  Pallas kernels  41 us (28%)
  between operations  13.4 us (9%)
  local copies, waits for them, and re-layouts  3.08 us (2%)
    all_gather x1, waiting for transfers between devices, local(): pool_weight = lax.all_gather(pool_weight, 'sp', axis=2, tiled=True)  87.7 us
    pallas_call x1, Pallas kernels, local(): pl.pallas_call(functools.partial(kernel, (layers, rows, width, shard_rows...  41 us
    unnamed x1, local copies, waits for them, and re-layouts  3.08 us
  transfers between devices with their start and end apart: 1, of which 1 were waited for; matrix products, arithmetic and copies ran while one was open for 0% of the time, Pallas kernels for 0%

commit v1 on v0

v1 whole, which is shorter than its diff:
```python
import functools

import jax
import jax.numpy as jnp
from jax import lax
from jax.experimental import pallas as pl
from jax.experimental.pallas import tpu as pltpu
from jax.sharding import PartitionSpec as P

D = 4096
POOL_GROUPS = 4
NORM_EPS = 1e-06
PAD = 64
HALO = 32
TILE = 128
WINDOW = TILE + 2 * PAD
NY = 4
STAGGER = 3
ROUNDS = 6
ALONG_Z, ALONG_Y, ACROSS = 0, 1, 2
MESH = pl.DeviceIdType.MESH


def kernel(cfg, x_hbm, w_hbm, gain_hbm, scale_hbm, out_ref, gain_ref, scale_ref, xs, ps, ws, band, fac_in, fac, ss_own, ss_in,
           load_sem, halo_send, halo_recv, ss_send, ss_recv, w_send, w_recv, out_sem):
    layers, rows, width, shard_rows, n_sp, n_tp = cfg
    sp, tp = lax.axis_index("sp"), lax.axis_index("tp")
    nz = n_sp // (2 * NY)
    z, y, c = sp // (2 * NY), (sp // 2) % NY, sp % 2
    tiles = (rows + 2 * PAD) // TILE
    seq_total = rows * n_sp
    base_pos = sp * rows - PAD
    half = jnp.left_shift(jnp.int32(1), tp)
    has_prev, has_next = sp > 0, sp < n_sp - 1

    x_load = pltpu.make_async_copy(x_hbm, xs.at[pl.ds(2 * PAD, rows)], load_sem.at[layers])
    w_loads = [pltpu.make_async_copy(w_hbm.at[l, 0], ws.at[l, z, y, c], load_sem.at[l]) for l in range(layers)]
    gain_load = pltpu.make_async_copy(gain_hbm, gain_ref, load_sem.at[layers + 1])
    scale_load = pltpu.make_async_copy(scale_hbm, scale_ref, load_sem.at[layers + 2])
    w_loads[0].start()
    x_load.start()
    for l in range(1, layers):
        w_loads[l].start()
    gain_load.start()
    scale_load.start()

    def at_z(step):
        return ((lax.rem(z + step + nz, nz) * NY + y) * 2 + c, tp)

    def at_y(step):
        return ((z * NY + lax.rem(y + step + NY, NY)) * 2 + c, tp)

    partner = ((z * NY + y) * 2 + 1 - c, tp)

    barrier = pltpu.get_barrier_semaphore()

    def greet(device):
        pl.semaphore_signal(barrier, inc=1, device_id=device, device_id_type=MESH)

    for device in [at_z(1), at_z(-1), at_y(1), at_y(-1), at_y(2), partner]:
        greet(device)
    for p in range(1, n_tp):
        greet((sp, lax.rem(tp + p, n_tp)))
    pl.when(has_prev)(lambda: greet((sp - 1, tp)))
    pl.when(has_next)(lambda: greet((sp + 1, tp)))
    expected = 6 + n_tp - 1 + has_prev.astype(jnp.int32) + has_next.astype(jnp.int32)

    zero = jnp.zeros((2 * PAD, width), jnp.bfloat16)
    xs[pl.ds(0, 2 * PAD - HALO)] = zero[: 2 * PAD - HALO]
    xs[pl.ds(2 * PAD + rows + HALO, 2 * PAD - HALO)] = zero[: 2 * PAD - HALO]

    @pl.when(jnp.logical_not(has_prev))
    def _():
        xs[pl.ds(2 * PAD - HALO, HALO)] = zero[:HALO]

    @pl.when(jnp.logical_not(has_next))
    def _():
        xs[pl.ds(2 * PAD + rows, HALO)] = zero[:HALO]

    ss_own[...] = jnp.zeros(ss_own.shape, jnp.float32)
    fac_in[...] = jnp.zeros(fac_in.shape, jnp.float32)

    pl.semaphore_wait(barrier, expected)

    to_next = pltpu.make_async_remote_copy(
        x_hbm.at[pl.ds(rows - HALO, HALO)], xs.at[pl.ds(2 * PAD - HALO, HALO)],
        halo_send.at[0], halo_recv.at[0], device_id=(sp + 1, tp), device_id_type=MESH)
    to_prev = pltpu.make_async_remote_copy(
        x_hbm.at[pl.ds(0, HALO)], xs.at[pl.ds(2 * PAD + rows, HALO)],
        halo_send.at[1], halo_recv.at[1], device_id=(sp - 1, tp), device_id_type=MESH)

    def start_halo():
        pl.when(has_next)(lambda: to_next.start())
        pl.when(has_prev)(lambda: to_prev.start())

    def zz(step):
        return lax.rem(z + step + nz, nz)

    def yy(step):
        return lax.rem(y + step + NY, NY)

    def shard_copy(l, dz, dy, device, way):
        zs, ys = zz(dz), yy(dy)
        piece = ws.at[l, zs, ys, c]
        return pltpu.make_async_remote_copy(
            piece, piece, w_send.at[l, way], w_recv.at[l, (zs * NY + ys) * 2 + c],
            device_id=device, device_id_type=MESH)

    def z_out(l, dz, dy, step):
        shard_copy(l, dz, dy, at_z(step), ALONG_Z).start()

    def y_out(l, dz):
        for step in (1, -1, 2):
            shard_copy(l, dz, 0, at_y(step), ALONG_Y).start()

    def got(l, dz, dy):
        shard_copy(l, dz, dy, partner, ALONG_Z).wait_recv()

    def slab_copy(l, zs, core):
        slab = ws.at[l, zs, :, core]
        return pltpu.make_async_remote_copy(
            slab, slab, w_send.at[l, ACROSS], w_recv.at[l, zs * NY * 2 + core],
            device_id=partner, device_id_type=MESH)

    def across(l, dz):
        slab_copy(l, zz(dz), c).start()

    def got_across(l):
        for zs in range(nz):
            slab_copy(l, zs, 1 - c).wait_recv()

    far = nz // 2

    def z_first(l, k):
        if k == 0:
            z_out(l, 0, 0, 1)
            z_out(l, 0, 0, -1)
            y_out(l, 0)
        if 1 <= k <= far:
            got(l, -k, 0)
            if k < far:
                z_out(l, -k, 0, 1)
            if k < far:
                got(l, k, 0)
                if k < far - 1:
                    z_out(l, k, 0, -1)
            y_out(l, -k)
            if k < far:
                y_out(l, k)
        if k >= 1:
            j = k - 1
            for dz in ([0] if j == 0 else [-j] if j == far else [-j, j]):
                for dy in (1, -1, 2):
                    got(l, dz, dy)
                across(l, dz)

    def z_hop(l, k, dy):
        up_far = dy in (0, 3)
        if k < far or up_far:
            got(l, -k, dy)
            if k < far - 1 or (k == far - 1 and up_far):
                z_out(l, -k, dy, 1)
        if k < far or not up_far:
            got(l, k, dy)
            if k < far - 1 or (k == far - 1 and not up_far):
                z_out(l, k, dy, -1)

    def y_first(l, k):
        if k == 0:
            y_out(l, 0)
            z_out(l, 0, 0, 1)
            z_out(l, 0, 0, -1)
        if k == 1:
            for dy in (1, 3):
                got(l, 0, dy)
                z_out(l, 0, dy, 1)
                z_out(l, 0, dy, -1)
            z_hop(l, 1, 0)
            got(l, 0, 2)
            z_out(l, 0, 2, 1)
            z_out(l, 0, 2, -1)
            across(l, 0)
        if k >= 2:
            if k <= far:
                z_hop(l, k, 0)
            for dy in (1, 3, 2):
                z_hop(l, k - 1, dy)
            j = k - 1
            for dz in ([-j] if j == far else [-j, j]):
                across(l, dz)

    def comm_round(l, k):
        if k == 0:
            w_loads[l].wait()
        pl.when(c == 0)(lambda: z_first(l, k))
        pl.when(c == 1)(lambda: y_first(l, k))

    def build_band():
        @pl.loop(0, tiles)
        def _(i):
            offset = (
                lax.broadcasted_iota(jnp.int32, (TILE, WINDOW), 1)
                - lax.broadcasted_iota(jnp.int32, (TILE, WINDOW), 0)
                - PAD
            )
            pos = base_pos + i * TILE + lax.broadcasted_iota(jnp.int32, (TILE, WINDOW), 0)
            count = jnp.minimum(pos + half, seq_total) - jnp.maximum(pos - half, 0)
            inverse = 1.0 / jnp.maximum(count, 1).astype(jnp.float32)
            mean = jnp.where((offset >= -half) & (offset < half), inverse, 0.0)
            band[i] = mean - jnp.where(offset == 0, 1.0, 0.0)

    def store_sums(layer, i, part):
        ss_own[layer, pl.ds(i, 1)] = jnp.sum(part.T, axis=0, keepdims=True)

    def square_sums():
        @pl.loop(0, tiles // 3)
        def _(b):
            for t in range(3):
                i = b * 3 + t
                part = jnp.zeros((TILE, 128), jnp.float32)
                for n in range(width // 128):
                    v = xs[pl.ds(pl.multiple_of(PAD + i * TILE, 64), TILE), pl.ds(n * 128, 128)].astype(jnp.float32)
                    part = part + v * v
                store_sums(0, i, part)

    def ss_copy(layer, p):
        return pltpu.make_async_remote_copy(
            ss_own.at[layer], ss_in.at[layer, p - 1], ss_send.at[layer, p - 1], ss_recv.at[layer, p - 1],
            device_id=(sp, lax.rem(tp + p, n_tp)), device_id_type=MESH)

    def send_sums(layer):
        for p in range(1, n_tp):
            ss_copy(layer, p).start()

    def factors(layer):
        for p in range(1, n_tp):
            ss_copy(layer, p).wait()
        total = ss_own[layer]
        for p in range(1, n_tp):
            total = total + ss_in[layer, p - 1]
        factor = lax.rsqrt(total / D + NORM_EPS)
        tile = lax.broadcasted_iota(jnp.int32, total.shape, 0)
        lane = lax.broadcasted_iota(jnp.int32, total.shape, 1)
        pos = base_pos + tile * TILE + lane
        factor = jnp.where((pos >= 0) & (pos < seq_total) & (tile < tiles), factor, 0.0)
        fac_in[pl.ds(8, 16)] = factor
        low = pltpu.roll(fac_in[pl.ds(7, 16)], PAD, 1)
        high = pltpu.roll(factor, PAD, 1)
        fac[...] = jnp.where(lane < PAD, low, high)

    def pool(layer, b):
        for t in range(3):
            i = b * 3 + t
            factor = jnp.concatenate([fac[i : i + 1], fac[i + 1 : i + 2]], axis=1)
            weights = (band[i] * factor).astype(jnp.bfloat16)
            for n in range(width // 256):
                cols = pl.ds(n * 256, 256)
                sums = jnp.dot(weights, xs[pl.ds(i * TILE, WINDOW), cols], preferred_element_type=jnp.float32)
                g = gain_ref[layer : layer + 1, cols].astype(jnp.float32)
                ps[pl.ds(i * TILE, TILE), cols] = (sums * g).astype(jnp.bfloat16)

    def mixed_block(layer, first_row, block, n):
        cols = pl.ds(n * 256, 256)
        weight = ws[layer, :, :, :, :, cols].reshape(width, 256)
        branch = jnp.dot(ps[pl.ds(first_row, block)], weight, preferred_element_type=jnp.float32)
        s = scale_ref[layer : layer + 1, cols].astype(jnp.float32)
        at = pl.ds(PAD + first_row, block)
        mixed = (xs[at, cols].astype(jnp.float32) + branch * s).astype(jnp.bfloat16)
        xs[at, cols] = mixed
        return mixed

    def mix(layer, b):
        block = 3 * TILE
        part = jnp.zeros((block, 128), jnp.float32)
        for n in range(width // 256):
            v = mixed_block(layer, b * block, block, n).astype(jnp.float32)
            sq = v * v
            part = part + sq[:, :128] + sq[:, 128:]
        for t in range(3):
            store_sums(layer + 1, b * 3 + t, part[t * TILE : (t + 1) * TILE])

    def start_work():
        x_load.wait()
        gain_load.wait()
        scale_load.wait()
        pl.when(has_prev)(lambda: to_next.wait_recv())
        pl.when(has_next)(lambda: to_prev.wait_recv())

    tasks = {}

    def do(t, *work):
        tasks.setdefault(t, []).extend(work)

    part = functools.partial
    do(0, start_halo, build_band)
    do(1, start_work, square_sums, part(send_sums, 0))
    do(2, part(factors, 0), part(pool, 0, 0))
    do(3, part(pool, 0, 1), part(pool, 0, 2))
    for layer in range(layers - 1):
        t = ROUNDS - 1 + STAGGER * layer
        do(t, part(got_across, layer), part(mix, layer, 0))
        do(t + 1, part(mix, layer, 1))
        do(t + 2, part(mix, layer, 2), part(send_sums, layer + 1))
        do(t + 3, part(factors, layer + 1), part(pool, layer + 1, 0), part(pool, layer + 1, 1), part(pool, layer + 1, 2))

    last = layers - 1
    for t in range(ROUNDS + STAGGER * last):
        for l in range(layers):
            if 0 <= t - STAGGER * l < ROUNDS:
                comm_round(l, t - STAGGER * l)
        for work in tasks.get(t, []):
            work()
    got_across(last)

    outs = []
    block = rows // 2
    for b in range(2):
        for n in range(width // 256):
            mixed_block(last, PAD + b * block, block, n)
            at, cols = pl.ds(2 * PAD + b * block, block), pl.ds(n * 256, 256)
            outs.append(pltpu.make_async_copy(
                xs.at[at, cols], out_ref.at[pl.ds(b * block, block), cols], out_sem.at[len(outs)]))
            outs[-1].start()

    pl.when(has_next)(lambda: to_next.wait_send())
    pl.when(has_prev)(lambda: to_prev.wait_send())

    def drain(l, way, refs):
        pltpu.make_async_remote_copy(
            refs, refs, w_send.at[l, way], w_recv.at[l, 0], device_id=partner, device_id_type=MESH).wait_send()

    for l in range(layers):
        drain(l, ACROSS, ws.at[l, :, :, 0])

        @pl.when(c == 0)
        def _():
            drain(l, ALONG_Z, ws.at[l, pl.ds(0, nz - 1), 0, 0])
            drain(l, ALONG_Y, ws.at[l, :, pl.ds(0, NY - 1), 0])

        @pl.when(c == 1)
        def _():
            drain(l, ALONG_Z, ws.at[l, pl.ds(0, nz - 1), :, 0])
            drain(l, ALONG_Y, ws.at[l, 0, pl.ds(0, NY - 1), 0])

    for out in outs:
        out.wait()


def solution(mesh):
    n_sp, n_tp = mesh.shape["sp"], mesh.shape["tp"]

    def local(stream, norm_gain, pool_weight, pool_scale):
        rows, _ = stream.shape
        layers, per_dev, shard_rows, width = pool_weight.shape
        assert per_dev == 1 and n_tp == POOL_GROUPS and n_sp % (4 * NY) == 0
        total_rows = rows + 2 * PAD
        dma = pltpu.SemaphoreType.DMA
        hbm = pl.BlockSpec(memory_space=pltpu.HBM)
        return pl.pallas_call(
            functools.partial(kernel, (layers, rows, width, shard_rows, n_sp, n_tp)),
            out_shape=jax.ShapeDtypeStruct((rows, width), jnp.bfloat16),
            in_specs=[hbm] * 4,
            out_specs=hbm,
            scratch_shapes=[
                pltpu.VMEM((layers, width), jnp.bfloat16),
                pltpu.VMEM((layers, width), jnp.bfloat16),
                pltpu.VMEM((total_rows + 2 * PAD, width), jnp.bfloat16),
                pltpu.VMEM((total_rows, width), jnp.bfloat16),
                pltpu.VMEM((layers, n_sp // (2 * NY), NY, 2, shard_rows, width), jnp.bfloat16),
                pltpu.VMEM((total_rows // TILE, TILE, WINDOW), jnp.float32),
                pltpu.VMEM((24, TILE), jnp.float32),
                pltpu.VMEM((16, TILE), jnp.float32),
                pltpu.VMEM((layers, 16, TILE), jnp.float32),
                pltpu.VMEM((layers, n_tp - 1, 16, TILE), jnp.float32),
                dma((layers + 3,)),
                dma((2,)),
                dma((2,)),
                dma((layers, n_tp - 1)),
                dma((layers, n_tp - 1)),
                dma((layers, 3)),
                dma((layers, n_sp)),
                dma((8,)),
            ],
            compiler_params=pltpu.CompilerParams(
                collective_id=0, has_side_effects=True, vmem_limit_bytes=60 * 2**20
            ),
        )(stream, pool_weight, norm_gain, pool_scale)

    placed = (P("sp", "tp"), P(None, "tp"), P(None, "tp", "sp", None), P(None, "tp"))
    return jax.shard_map(
        local, mesh=mesh, in_specs=placed, out_specs=P("sp", "tp"), check_vma=False
    )
```

time: 149 us -> 63.1 us (0.42); the launches traced: 146 us -> 63 us
  waiting for transfers between devices: 88.4 us -> 0 us
  Pallas kernels: 41 us -> 59.9 us
  between operations: 13.4 us -> 0.01 us
    all_gather x1 -> x0, waiting for transfers between devices: 87.7 us -> none  [local(): pool_weight = lax.all_gather(pool_weight, 'sp', axis=2, tiled=True)]
    pallas_call x1, Pallas kernels: 41 us -> 59.9 us  [local(): pl.pallas_call(functools.partial(kernel, (layers, rows, width, shard_rows...]
  transfers between devices with their start and end apart: 1 -> 0, of which waited for: 1 -> 0; matrix products, arithmetic and copies ran while one was open for 0% -> 0% of each run, Pallas kernels for 0% -> 0%
where the time goes in v1:
time: 63.1 us; the launch traced here: 63 us
  Pallas kernels  59.9 us (95%)
  local copies, waits for them, and re-layouts  3.08 us (5%)
    pallas_call x1, Pallas kernels, local(): pl.pallas_call(functools.partial(kernel, (layers, rows, width, shard_rows...  59.9 us
    unnamed x1, local copies, waits for them, and re-layouts  3.08 us

profile of v1, /device:TPU:1, one launch (start us, length us, event | category | flops | bytes accessed | tf_op | source)
XLA Modules:
  0.0 63.0 jit_solution(15596086340288638423)
XLA Ops:
  0.0 59.9 %shard_map.46 = bf16[1024,1024]{1,0:T(8,128)(2,1)} custom-call(bf16[1024,1024]{1,0:T(8,128)(2,1)} %x_hbm.1, bf16[3,1,16,1024]{3,2,1,0:T(8,128)(2,1)} %w_hbm.1, bf16[3,1024]{1,0:T(4,128)(2,1)} %gain_hbm.1, bf16[3,1024]{1,0:T(4,128)(2,1)} %scale_hbm.1), custom_call_target="tpu_custom_call" | custom-call | tf_op jit(solution)/shard_map/pallas_call | solution.py:359
  59.9 3.1 %copy.6 = bf16[1024,1024]{1,0:T(8,128)(2,1)} copy(bf16[1024,1024]{1,0:T(8,128)(2,1)} %shard_map.46) | data formatting | bytes 4194304

commit v2 on v1

v2 whole, which is shorter than its diff:
```python
import functools

import jax
import jax.numpy as jnp
from jax import lax
from jax.experimental import pallas as pl
from jax.experimental.pallas import tpu as pltpu
from jax.sharding import PartitionSpec as P

D = 4096
POOL_GROUPS = 4
NORM_EPS = 1e-06
PAD = 64
HALO = 32
TILE = 128
WINDOW = TILE + 2 * PAD
PER = 3
BLOCKS = 3
NY = 4
FAST = (False, False, False)
PLAN = (
    ((30, 130, 20, 40, 31, 33), (30, 130, 20, 40, 33, 31), 'x00'),
    ((32, 120, 140, 131, 133, 230, 10, 21, 23, 132, 50, 43, 41, 22), (32, 120, 133, 131, 10, 50, 140, 230, 43, 23, 21, 41, 132, 22, 42, 143), 'q00'),
    ((42, 110, 150, 121, 123, 141, 143), (110, 123, 141, 60, 121), 'q01'),
    ((122, 231, 233), (0, 150, 231, 233, 220, 240), 'q02'),
    ((142, 220, 11, 13, 240, 232, 0, 53, 51, 60, 12, 113, 111, 52, 100, 153, 151, 160, 112, 223, 221, 152, 243, 241, 3, 1, 222, 210, 250, 242, 63, 61, 2, 70, 103, 101, 62, 163, 161, 102, 213, 211, 170, 162, 253, 251, 212, 260, 71, 73, 252, 200, 72), (13, 51, 53, 232, 11, 142, 122, 12, 52, 100, 153, 151, 113, 111, 160, 70, 241, 221, 243, 223, 250, 210, 61, 63, 3, 222, 242, 1, 152, 62, 112, 163, 2, 161, 170, 251, 103, 253, 260, 101, 71, 211, 252, 213, 200, 162, 73, 72, 171, 212, 261, 102, 263, 173, 262, 201, 172, 203), 'm00'),
    ((171, 173), (270, 202, 271), 'm01'),
    ((172, 261, 263), (273, 272), 'm02'),
    ((270, 201, 203, 262, 202, 273, 271), (), 'q10'),
    ((), (), 'm10'),
    ((272,), (), 'q11'),
    ((), (), 'm11'),
    ((), (), 'q12'),
    ((), (), 'm12'),
    ((), (), 'q20'),
    ((), (), 'm20'),
    ((), (), 'q21'),
    ((), (), 'm21'),
    ((), (), 'q22'),
    ((), (), 'm22'),
    ((), (), ''),
)
ALONG_Z, ALONG_Y, ACROSS = 0, 1, 2
MESH = pl.DeviceIdType.MESH


def kernel(cfg, x_hbm, w_hbm, gain_hbm, scale_hbm, out_ref, gain_ref, scale_ref, xs, ps, ws, band, fac, ss_own, ss_in,
           load_sem, halo_send, halo_recv, ss_send, ss_recv, w_send, w_recv):
    layers, rows, width, shard_rows, n_sp, n_tp = cfg
    sp, tp = lax.axis_index("sp"), lax.axis_index("tp")
    nz = n_sp // (2 * NY)
    z, y, c = sp // (2 * NY), (sp // 2) % NY, sp % 2
    tiles = (rows + 2 * PAD) // TILE
    seq_total = rows * n_sp
    base_pos = sp * rows - PAD
    half = jnp.left_shift(jnp.int32(1), tp)
    has_prev, has_next = sp > 0, sp < n_sp - 1

    x_load = pltpu.make_async_copy(x_hbm, xs.at[0, pl.ds(2 * PAD, rows)], load_sem.at[layers])
    w_loads = [pltpu.make_async_copy(w_hbm.at[l, 0], ws.at[l, z, y, c], load_sem.at[l]) for l in range(layers)]
    gain_load = pltpu.make_async_copy(gain_hbm, gain_ref, load_sem.at[layers + 1])
    scale_load = pltpu.make_async_copy(scale_hbm, scale_ref, load_sem.at[layers + 2])
    w_loads[0].start()
    x_load.start()
    for l in range(1, layers):
        w_loads[l].start()
    gain_load.start()
    scale_load.start()

    def at_z(step):
        return ((lax.rem(z + step + nz, nz) * NY + y) * 2 + c, tp)

    def at_y(step):
        return ((z * NY + lax.rem(y + step + NY, NY)) * 2 + c, tp)

    partner = ((z * NY + y) * 2 + 1 - c, tp)

    barrier = pltpu.get_barrier_semaphore()

    def greet(device):
        pl.semaphore_signal(barrier, inc=1, device_id=device, device_id_type=MESH)

    for device in [at_z(1), at_z(-1), at_y(1), at_y(-1), at_y(2), partner]:
        greet(device)
    for p in range(1, n_tp):
        greet((sp, lax.rem(tp + p, n_tp)))
    pl.when(has_prev)(lambda: greet((sp - 1, tp)))
    pl.when(has_next)(lambda: greet((sp + 1, tp)))
    expected = 6 + n_tp - 1 + has_prev.astype(jnp.int32) + has_next.astype(jnp.int32)

    zero = jnp.zeros((2 * PAD, width), jnp.bfloat16)
    xs[0, pl.ds(0, 2 * PAD - HALO)] = zero[: 2 * PAD - HALO]
    xs[0, pl.ds(2 * PAD + rows + HALO, 2 * PAD - HALO)] = zero[: 2 * PAD - HALO]
    xs[1, pl.ds(0, PAD)] = zero[:PAD]
    xs[1, pl.ds(3 * PAD + rows, PAD)] = zero[:PAD]

    @pl.when(jnp.logical_not(has_prev))
    def _():
        xs[0, pl.ds(2 * PAD - HALO, HALO)] = zero[:HALO]

    @pl.when(jnp.logical_not(has_next))
    def _():
        xs[0, pl.ds(2 * PAD + rows, HALO)] = zero[:HALO]

    ss_own[...] = jnp.zeros(ss_own.shape, jnp.float32)
    fac[...] = jnp.zeros(fac.shape, jnp.float32)

    pl.semaphore_wait(barrier, expected)

    to_next = pltpu.make_async_remote_copy(
        x_hbm.at[pl.ds(rows - HALO, HALO)], xs.at[0, pl.ds(2 * PAD - HALO, HALO)],
        halo_send.at[0], halo_recv.at[0], device_id=(sp + 1, tp), device_id_type=MESH)
    to_prev = pltpu.make_async_remote_copy(
        x_hbm.at[pl.ds(0, HALO)], xs.at[0, pl.ds(2 * PAD + rows, HALO)],
        halo_send.at[1], halo_recv.at[1], device_id=(sp - 1, tp), device_id_type=MESH)

    def start_halo():
        pl.when(has_next)(lambda: to_next.start())
        pl.when(has_prev)(lambda: to_prev.start())

    def zz(step):
        return lax.rem(z + step + nz, nz)

    def yy(step):
        return lax.rem(y + step + NY, NY)

    def shard_copy(l, dz, dy, device, way):
        zs, ys = zz(dz), yy(dy)
        piece = ws.at[l, zs, ys, c]
        return pltpu.make_async_remote_copy(
            piece, piece, w_send.at[l, way], w_recv.at[l, (zs * NY + ys) * 2 + c],
            device_id=device, device_id_type=MESH)

    def z_out(l, dz, dy, step):
        shard_copy(l, dz, dy, at_z(step), ALONG_Z).start()

    def y_out(l, dz):
        for step in (1, -1, 2):
            shard_copy(l, dz, 0, at_y(step), ALONG_Y).start()

    def got(l, dz, dy):
        shard_copy(l, dz, dy, partner, ALONG_Z).wait_recv()

    def slab_copy(l, zs, core):
        slab = ws.at[l, zs, :, core]
        return pltpu.make_async_remote_copy(
            slab, slab, w_send.at[l, ACROSS], w_recv.at[l, zs * NY * 2 + core],
            device_id=partner, device_id_type=MESH)

    def across(l, dz):
        slab_copy(l, zz(dz), c).start()

    def got_across(l):
        for zs in range(nz):
            slab_copy(l, zs, 1 - c).wait_recv()

    far = nz // 2

    def goes_up(dy):
        return dy in (0, 3)

    def z_steps(l, dz, dy, up):
        if FAST[l]:
            return {0: (2, -2, 1, -1), -2: (2, 1) if up else (1,), 2: (-1,) if up else (-2, -1)}.get(dz, ())
        if dz == 0:
            return (1, -1)
        if dz < 0:
            return (1,) if -dz < far - 1 + up else ()
        return (-1,) if dz < far - up else ()

    seen = {}

    def pass_on(core, event):
        l, dz, dy = event // 100, event // 10 % 10 - 3, event % 10
        if (dz, dy) == (0, 0):
            w_loads[l].wait()
        else:
            got(l, dz, dy)
        if core == 0:
            if dy == 0:
                for step in z_steps(l, dz, dy, 1):
                    z_out(l, dz, dy, step)
                y_out(l, dz)
        else:
            if (dz, dy) == (0, 0):
                y_out(l, dz)
            for step in z_steps(l, dz, dy, int(goes_up(dy))):
                z_out(l, dz, dy, step)
        seen[core, l, dz] = seen.get((core, l, dz), 0) + 1
        if seen[core, l, dz] == NY:
            across(l, dz)

    def pass_all(core, events):
        for event in events:
            pass_on(core, event)

    def build_band():
        @pl.loop(0, tiles)
        def _(i):
            offset = (
                lax.broadcasted_iota(jnp.int32, (TILE, WINDOW), 1)
                - lax.broadcasted_iota(jnp.int32, (TILE, WINDOW), 0)
                - PAD
            )
            pos = base_pos + i * TILE + lax.broadcasted_iota(jnp.int32, (TILE, WINDOW), 0)
            count = jnp.minimum(pos + half, seq_total) - jnp.maximum(pos - half, 0)
            inverse = 1.0 / jnp.maximum(count, 1).astype(jnp.float32)
            mean = jnp.where((offset >= -half) & (offset < half), inverse, 0.0)
            band[i] = mean - jnp.where(offset == 0, 1.0, 0.0)

    def store_sums(layer, b, t, part):
        ss_own[layer, b, pl.ds(t, 1)] = jnp.sum(part.T, axis=0, keepdims=True)

    def square_sums():
        @pl.loop(0, BLOCKS)
        def _(b):
            for t in range(PER):
                row = pl.multiple_of(PAD + b * (PER * TILE), 64) + t * TILE
                part = jnp.zeros((TILE, 128), jnp.float32)
                for n in range(width // 128):
                    v = xs[0, pl.ds(row, TILE), pl.ds(n * 128, 128)].astype(jnp.float32)
                    part = part + v * v
                store_sums(0, b, t, part)

    def ss_copy(layer, b, p):
        return pltpu.make_async_remote_copy(
            ss_own.at[layer, b], ss_in.at[layer, p - 1, b], ss_send.at[layer, p - 1, b], ss_recv.at[layer, p - 1, b],
            device_id=(sp, lax.rem(tp + p, n_tp)), device_id_type=MESH)

    def send_sums(layer, b):
        for p in range(1, n_tp):
            ss_copy(layer, b, p).start()

    def factors(layer, b):
        for p in range(1, n_tp):
            ss_copy(layer, b, p).wait()
        total = ss_own[layer, b]
        for p in range(1, n_tp):
            total = total + ss_in[layer, p - 1, b]
        factor = lax.rsqrt(total / D + NORM_EPS)
        tile = b * PER + lax.broadcasted_iota(jnp.int32, total.shape, 0)
        pos = base_pos + tile * TILE + lax.broadcasted_iota(jnp.int32, total.shape, 1)
        factor = jnp.where((pos >= 0) & (pos < seq_total), factor, 0.0)
        fac[pl.ds(8 + b * PER, PER)] = factor[:PER]

    def pool(layer, b):
        low = pltpu.roll(fac[pl.ds(7 + b * PER, PER + 1)], PAD, 1)
        high = pltpu.roll(fac[pl.ds(8 + b * PER, PER + 1)], PAD, 1)
        lane = lax.broadcasted_iota(jnp.int32, low.shape, 1)
        shifted = jnp.where(lane < PAD, low, high)
        for t in range(PER):
            i = b * PER + t
            factor = jnp.concatenate([shifted[t : t + 1], shifted[t + 1 : t + 2]], axis=1)
            weights = (band[i] * factor).astype(jnp.bfloat16)
            for n in range(width // 256):
                cols = pl.ds(n * 256, 256)
                window = xs[layer % 2, pl.ds(i * TILE, WINDOW), cols]
                sums = jnp.dot(weights, window, preferred_element_type=jnp.float32)
                g = gain_ref[layer : layer + 1, cols].astype(jnp.float32)
                ps[pl.ds(i * TILE, TILE), cols] = (sums * g).astype(jnp.bfloat16)

    def mixed_block(layer, first_row, block, n):
        cols = pl.ds(n * 256, 256)
        weight = ws[layer, :, :, :, :, cols].reshape(width, 256)
        branch = jnp.dot(ps[pl.ds(first_row, block)], weight, preferred_element_type=jnp.float32)
        s = scale_ref[layer : layer + 1, cols].astype(jnp.float32)
        old = xs[layer % 2, pl.ds(PAD + first_row, block), cols].astype(jnp.float32)
        return (old + branch * s).astype(jnp.bfloat16)

    def mix(layer, b):
        block = PER * TILE
        part = jnp.zeros((block, 128), jnp.float32)
        for n in range(width // 256):
            mixed = mixed_block(layer, b * block, block, n)
            xs[(layer + 1) % 2, pl.ds(PAD + b * block, block), pl.ds(n * 256, 256)] = mixed
            v = mixed.astype(jnp.float32)
            sq = v * v
            part = part + sq[:, :128] + sq[:, 128:]
        for t in range(PER):
            store_sums(layer + 1, b, t, part[t * TILE : (t + 1) * TILE])
        send_sums(layer + 1, b)

    def mix_out(layer, b):
        first = max(b * PER * TILE, PAD)
        block = min((b + 1) * PER * TILE, PAD + rows) - first
        for n in range(width // 256):
            out_ref[pl.ds(first - PAD, block), pl.ds(n * 256, 256)] = mixed_block(layer, first, block, n)

    def start_work():
        x_load.wait()
        gain_load.wait()
        scale_load.wait()
        pl.when(has_prev)(lambda: to_next.wait_recv())
        pl.when(has_next)(lambda: to_prev.wait_recv())

    last = layers - 1

    def task(name):
        kind, l, b = name[0], int(name[1]), int(name[2])
        if kind == "x":
            start_work()
            square_sums()
            for block in range(BLOCKS):
                send_sums(0, block)
        elif kind == "q":
            if b == 0:
                factors(l, 0)
            if b < BLOCKS - 1:
                factors(l, b + 1)
            pool(l, b)
        elif kind == "m":
            if b == 0:
                got_across(l)
            (mix_out if l == last else mix)(l, b)

    for l in range(layers):
        if l * 100 + 30 in PLAN[0][0]:
            pl.when(c == 0)(functools.partial(pass_on, 0, l * 100 + 30))
            pl.when(c == 1)(functools.partial(pass_on, 1, l * 100 + 30))
    start_halo()
    build_band()
    for first, second, name in PLAN:
        if name == "x00":
            first = [e for e in first if e % 100 != 30]
            second = [e for e in second if e % 100 != 30]
        if first:
            pl.when(c == 0)(functools.partial(pass_all, 0, first))
        if second:
            pl.when(c == 1)(functools.partial(pass_all, 1, second))
        if name:
            task(name)
    pl.when(has_next)(lambda: to_next.wait_send())
    pl.when(has_prev)(lambda: to_prev.wait_send())

    def drain(l, way, refs):
        pltpu.make_async_remote_copy(
            refs, refs, w_send.at[l, way], w_recv.at[l, 0], device_id=partner, device_id_type=MESH).wait_send()

    for l in range(layers):
        drain(l, ACROSS, ws.at[l, :, :, 0])

        @pl.when(c == 0)
        def _():
            drain(l, ALONG_Z, ws.at[l, pl.ds(0, nz - 1), 0, 0])
            drain(l, ALONG_Y, ws.at[l, :, pl.ds(0, NY - 1), 0])

        @pl.when(c == 1)
        def _():
            drain(l, ALONG_Z, ws.at[l, pl.ds(0, nz - 1), :, 0])
            drain(l, ALONG_Y, ws.at[l, 0, pl.ds(0, NY - 1), 0])


def solution(mesh):
    n_sp, n_tp = mesh.shape["sp"], mesh.shape["tp"]

    def local(stream, norm_gain, pool_weight, pool_scale):
        rows, _ = stream.shape
        layers, per_dev, shard_rows, width = pool_weight.shape
        assert per_dev == 1 and n_tp == POOL_GROUPS and n_sp % (4 * NY) == 0
        total_rows = rows + 2 * PAD
        dma = pltpu.SemaphoreType.DMA
        hbm = pl.BlockSpec(memory_space=pltpu.HBM)
        return pl.pallas_call(
            functools.partial(kernel, (layers, rows, width, shard_rows, n_sp, n_tp)),
            out_shape=pltpu.VMEM((rows, width), jnp.bfloat16),
            in_specs=[hbm] * 4,
            out_specs=pl.BlockSpec(memory_space=pltpu.VMEM),
            scratch_shapes=[
                pltpu.VMEM((layers, width), jnp.bfloat16),
                pltpu.VMEM((layers, width), jnp.bfloat16),
                pltpu.VMEM((2, total_rows + 2 * PAD, width), jnp.bfloat16),
                pltpu.VMEM((total_rows, width), jnp.bfloat16),
                pltpu.VMEM((layers, n_sp // (2 * NY), NY, 2, shard_rows, width), jnp.bfloat16),
                pltpu.VMEM((total_rows // TILE, TILE, WINDOW), jnp.float32),
                pltpu.VMEM((24, TILE), jnp.float32),
                pltpu.VMEM((layers, BLOCKS, 8, TILE), jnp.float32),
                pltpu.VMEM((layers, n_tp - 1, BLOCKS, 8, TILE), jnp.float32),
                dma((layers + 3,)),
                dma((2,)),
                dma((2,)),
                dma((layers, n_tp - 1, BLOCKS)),
                dma((layers, n_tp - 1, BLOCKS)),
                dma((layers, 3)),
                dma((layers, n_sp)),
            ],
            compiler_params=pltpu.CompilerParams(
                collective_id=0, has_side_effects=True, vmem_limit_bytes=60 * 2**20
            ),
        )(stream, pool_weight, norm_gain, pool_scale)

    placed = (P("sp", "tp"), P(None, "tp"), P(None, "tp", "sp", None), P(None, "tp"))
    return jax.shard_map(
        local, mesh=mesh, in_specs=placed, out_specs=P("sp", "tp"), check_vma=False
    )
```

time: 63.1 us -> 51.5 us (0.82)
  Pallas kernels: 59.9 us -> 49.6 us
  local copies, waits for them, and re-layouts: 3.08 us -> 1.32 us
    pallas_call x1, Pallas kernels: 59.9 us -> 49.6 us  [local(): pl.pallas_call(functools.partial(kernel, (layers, rows, width, shard_rows...]
    unnamed x1, local copies, waits for them, and re-layouts: 3.08 us -> 1.32 us
where the time goes in v2:
time: 51.5 us; the launch traced here: 50.9 us
  Pallas kernels  49.6 us (96%)
  local copies, waits for them, and re-layouts  1.32 us (3%)
    pallas_call x1, Pallas kernels, local(): pl.pallas_call(functools.partial(kernel, (layers, rows, width, shard_rows...  49.6 us
    unnamed x1, local copies, waits for them, and re-layouts  1.32 us

profile of v2, /device:TPU:1, one launch (start us, length us, event | category | flops | bytes accessed | tf_op | source)
XLA Modules:
  0.0 50.9 jit_solution(17918113416795128674)
XLA Ops:
  0.0 49.6 %shard_map.46 = bf16[1024,1024]{1,0:T(8,128)(2,1)S(1)} custom-call(bf16[1024,1024]{1,0:T(8,128)(2,1)} %x_hbm.1, bf16[3,1,16,1024]{3,2,1,0:T(8,128)(2,1)} %w_hbm.1, bf16[3,1024]{1,0:T(4,128)(2,1)} %gain_hbm.1, bf16[3,1024]{1,0:T(4,128)(2,1)} %scale_hbm.1), custom_call_target="tpu_custom_call" | custom-call | tf_op jit(solution)/shard_map/pallas_call | solution.py:363
  49.6 1.3 %copy.6 = bf16[1024,1024]{1,0:T(8,128)(2,1)} copy(bf16[1024,1024]{1,0:T(8,128)(2,1)S(1)} %shard_map.46) | data formatting | bytes 4194304

commit v3 on v2

--- a/solution.py
+++ b/solution.py
@@ -19,14 +19,15 @@
 NY = 4
 FAST = (False, False, False)
 PLAN = (
-    ((30, 130, 20, 40, 31, 33), (30, 130, 20, 40, 33, 31), 'x00'),
-    ((32, 120, 140, 131, 133, 230, 10, 21, 23, 132, 50, 43, 41, 22), (32, 120, 133, 131, 10, 50, 140, 230, 43, 23, 21, 41, 132, 22, 42, 143), 'q00'),
-    ((42, 110, 150, 121, 123, 141, 143), (110, 123, 141, 60, 121), 'q01'),
-    ((122, 231, 233), (0, 150, 231, 233, 220, 240), 'q02'),
-    ((142, 220, 11, 13, 240, 232, 0, 53, 51, 60, 12, 113, 111, 52, 100, 153, 151, 160, 112, 223, 221, 152, 243, 241, 3, 1, 222, 210, 250, 242, 63, 61, 2, 70, 103, 101, 62, 163, 161, 102, 213, 211, 170, 162, 253, 251, 212, 260, 71, 73, 252, 200, 72), (13, 51, 53, 232, 11, 142, 122, 12, 52, 100, 153, 151, 113, 111, 160, 70, 241, 221, 243, 223, 250, 210, 61, 63, 3, 222, 242, 1, 152, 62, 112, 163, 2, 161, 170, 251, 103, 253, 260, 101, 71, 211, 252, 213, 200, 162, 73, 72, 171, 212, 261, 102, 263, 173, 262, 201, 172, 203), 'm00'),
-    ((171, 173), (270, 202, 271), 'm01'),
-    ((172, 261, 263), (273, 272), 'm02'),
-    ((270, 201, 203, 262, 202, 273, 271), (), 'q10'),
+    ((30,), (30,), 'b00'),
+    ((20, 40, 31, 33, 130), (20, 40, 33, 31, 130), 'x00'),
+    ((32, 23, 21, 10, 43, 41, 50, 230, 22, 120, 140, 131, 133), (32, 10, 50, 43, 23, 21, 41, 230, 131, 133, 120, 22, 42, 140), 'q00'),
+    ((42, 132), (0, 13, 53, 60, 132, 51), 'q01'),
+    ((13, 11), (11,), 'q02'),
+    ((0, 60, 51, 53, 220, 240, 12, 231, 233, 52, 110, 232, 123, 121, 150, 143, 141, 122, 142, 3, 1, 70, 61, 63, 250, 223, 221, 2, 210, 243, 241, 62, 222, 113, 111, 242, 100, 160, 153, 151, 112, 73, 71, 152, 253, 251, 260, 213, 211, 72, 200, 252, 103, 101, 212, 163, 161), (220, 240, 121, 141, 231, 233, 143, 123, 110, 52, 232, 12, 150, 70, 63, 3, 142, 122, 61, 1, 250, 210, 151, 241, 111, 243, 221, 153, 223, 62, 113, 242, 100, 160, 222, 152, 2, 71, 73, 260, 112, 161, 200, 101, 251, 253, 211, 163, 213, 72, 103, 252), 'm00'),
+    ((170, 102, 162, 201, 203, 261, 263), (162, 170, 102, 171, 212, 261, 263, 270), 'm01'),
+    ((270, 202, 262), (203, 262, 201, 173), 'm02'),
+    ((171, 173, 172, 273, 271), (172, 202, 271, 273, 272), 'q10'),
     ((), (), 'm10'),
     ((272,), (), 'q11'),
     ((), (), 'm11'),
@@ -297,7 +298,10 @@
 
     def task(name):
         kind, l, b = name[0], int(name[1]), int(name[2])
-        if kind == "x":
+        if kind == "b":
+            start_halo()
+            build_band()
+        elif kind == "x":
             start_work()
             square_sums()
             for block in range(BLOCKS):
@@ -313,16 +317,7 @@
                 got_across(l)
             (mix_out if l == last else mix)(l, b)
 
-    for l in range(layers):
-        if l * 100 + 30 in PLAN[0][0]:
-            pl.when(c == 0)(functools.partial(pass_on, 0, l * 100 + 30))
-            pl.when(c == 1)(functools.partial(pass_on, 1, l * 100 + 30))
-    start_halo()
-    build_band()
     for first, second, name in PLAN:
-        if name == "x00":
-            first = [e for e in first if e % 100 != 30]
-            second = [e for e in second if e % 100 != 30]
         if first:
             pl.when(c == 0)(functools.partial(pass_all, 0, first))
         if second:

time: 51.5 us -> 51 us (level)
  no operation moved by 1% of the time
where the time goes in v3:
time: 51 us; the launch traced here: 50.6 us
  Pallas kernels  49.3 us (97%)
  local copies, waits for them, and re-layouts  1.32 us (3%)
    pallas_call x1, Pallas kernels, local(): pl.pallas_call(functools.partial(kernel, (layers, rows, width, shard_rows...  49.3 us
    unnamed x1, local copies, waits for them, and re-layouts  1.32 us

profile of v3, /device:TPU:1, one launch (start us, length us, event | category | flops | bytes accessed | tf_op | source)
XLA Modules:
  0.0 50.6 jit_solution(2044162029874460812)
XLA Ops:
  0.0 49.3 %shard_map.46 = bf16[1024,1024]{1,0:T(8,128)(2,1)S(1)} custom-call(bf16[1024,1024]{1,0:T(8,128)(2,1)} %x_hbm.1, bf16[3,1,16,1024]{3,2,1,0:T(8,128)(2,1)} %w_hbm.1, bf16[3,1024]{1,0:T(4,128)(2,1)} %gain_hbm.1, bf16[3,1024]{1,0:T(4,128)(2,1)} %scale_hbm.1), custom_call_target="tpu_custom_call" | custom-call | tf_op jit(solution)/shard_map/pallas_call | solution.py:358
  49.3 1.3 %copy.6 = bf16[1024,1024]{1,0:T(8,128)(2,1)} copy(bf16[1024,1024]{1,0:T(8,128)(2,1)S(1)} %shard_map.46) | data formatting | bytes 4194304

commit v4 on v3

--- a/solution.py
+++ b/solution.py
@@ -136,7 +136,7 @@
         shard_copy(l, dz, dy, at_z(step), ALONG_Z).start()
 
     def y_out(l, dz):
-        for step in (1, -1, 2):
+        for step in (2, 1, -1):
             shard_copy(l, dz, 0, at_y(step), ALONG_Y).start()
 
     def got(l, dz, dy):

time: 51 us -> 51.7 us (1.014)
  Pallas kernels: 49.3 us -> 50 us
    pallas_call x1, Pallas kernels: 49.3 us -> 50 us  [local(): pl.pallas_call(functools.partial(kernel, (layers, rows, width, shard_rows...]
where the time goes in v4:
time: 51.7 us; the launch traced here: 51.3 us
  Pallas kernels  50 us (97%)
  local copies, waits for them, and re-layouts  1.32 us (3%)
    pallas_call x1, Pallas kernels, local(): pl.pallas_call(functools.partial(kernel, (layers, rows, width, shard_rows...  50 us
    unnamed x1, local copies, waits for them, and re-layouts  1.32 us

profile of v4, /device:TPU:1, one launch (start us, length us, event | category | flops | bytes accessed | tf_op | source)
XLA Modules:
  0.0 51.3 jit_solution(16489926175509687638)
XLA Ops:
  0.0 50.0 %shard_map.46 = bf16[1024,1024]{1,0:T(8,128)(2,1)S(1)} custom-call(bf16[1024,1024]{1,0:T(8,128)(2,1)} %x_hbm.1, bf16[3,1,16,1024]{3,2,1,0:T(8,128)(2,1)} %w_hbm.1, bf16[3,1024]{1,0:T(4,128)(2,1)} %gain_hbm.1, bf16[3,1024]{1,0:T(4,128)(2,1)} %scale_hbm.1), custom_call_target="tpu_custom_call" | custom-call | tf_op jit(solution)/shard_map/pallas_call | solution.py:358
  50.0 1.3 %copy.6 = bf16[1024,1024]{1,0:T(8,128)(2,1)} copy(bf16[1024,1024]{1,0:T(8,128)(2,1)S(1)} %shard_map.46) | data formatting | bytes 4194304

commit v5 on v3

--- a/solution.py
+++ b/solution.py
@@ -106,6 +106,21 @@
     ss_own[...] = jnp.zeros(ss_own.shape, jnp.float32)
     fac[...] = jnp.zeros(fac.shape, jnp.float32)
 
+    def build_band():
+        @pl.loop(0, tiles)
+        def _(i):
+            offset = (
+                lax.broadcasted_iota(jnp.int32, (TILE, WINDOW), 1)
+                - lax.broadcasted_iota(jnp.int32, (TILE, WINDOW), 0)
+                - PAD
+            )
+            pos = base_pos + i * TILE + lax.broadcasted_iota(jnp.int32, (TILE, WINDOW), 0)
+            count = jnp.minimum(pos + half, seq_total) - jnp.maximum(pos - half, 0)
+            inverse = 1.0 / jnp.maximum(count, 1).astype(jnp.float32)
+            mean = jnp.where((offset >= -half) & (offset < half), inverse, 0.0)
+            band[i] = mean - jnp.where(offset == 0, 1.0, 0.0)
+
+    build_band()
     pl.semaphore_wait(barrier, expected)
 
     to_next = pltpu.make_async_remote_copy(
@@ -195,20 +210,6 @@
         for event in events:
             pass_on(core, event)
 
-    def build_band():
-        @pl.loop(0, tiles)
-        def _(i):
-            offset = (
-                lax.broadcasted_iota(jnp.int32, (TILE, WINDOW), 1)
-                - lax.broadcasted_iota(jnp.int32, (TILE, WINDOW), 0)
-                - PAD
-            )
-            pos = base_pos + i * TILE + lax.broadcasted_iota(jnp.int32, (TILE, WINDOW), 0)
-            count = jnp.minimum(pos + half, seq_total) - jnp.maximum(pos - half, 0)
-            inverse = 1.0 / jnp.maximum(count, 1).astype(jnp.float32)
-            mean = jnp.where((offset >= -half) & (offset < half), inverse, 0.0)
-            band[i] = mean - jnp.where(offset == 0, 1.0, 0.0)
-
     def store_sums(layer, b, t, part):
         ss_own[layer, b, pl.ds(t, 1)] = jnp.sum(part.T, axis=0, keepdims=True)
 
@@ -300,7 +301,6 @@
         kind, l, b = name[0], int(name[1]), int(name[2])
         if kind == "b":
             start_halo()
-            build_band()
         elif kind == "x":
             start_work()
             square_sums()

time: 51 us -> 51 us (level)
  no operation moved by 1% of the time
where the time goes in v5:
time: 51 us; the launch traced here: 50.6 us
  Pallas kernels  49.3 us (97%)
  local copies, waits for them, and re-layouts  1.32 us (3%)
    pallas_call x1, Pallas kernels, local(): pl.pallas_call(functools.partial(kernel, (layers, rows, width, shard_rows...  49.3 us
    unnamed x1, local copies, waits for them, and re-layouts  1.32 us

profile of v5, /device:TPU:1, one launch (start us, length us, event | category | flops | bytes accessed | tf_op | source)
XLA Modules:
  0.0 50.6 jit_solution(5862528278712186227)
XLA Ops:
  0.0 49.3 %shard_map.46 = bf16[1024,1024]{1,0:T(8,128)(2,1)S(1)} custom-call(bf16[1024,1024]{1,0:T(8,128)(2,1)} %x_hbm.1, bf16[3,1,16,1024]{3,2,1,0:T(8,128)(2,1)} %w_hbm.1, bf16[3,1024]{1,0:T(4,128)(2,1)} %gain_hbm.1, bf16[3,1024]{1,0:T(4,128)(2,1)} %scale_hbm.1), custom_call_target="tpu_custom_call" | custom-call | tf_op jit(solution)/shard_map/pallas_call | solution.py:358
  49.3 1.3 %copy.6 = bf16[1024,1024]{1,0:T(8,128)(2,1)} copy(bf16[1024,1024]{1,0:T(8,128)(2,1)S(1)} %shard_map.46) | data formatting | bytes 4194304
